TPU v7x, 768 devices: a whole 4x8x12 slice. The times are simulated.
768 devices in a mesh: ep: 24 (over z, core), tp: 32 (over y, x).
Axes of the slice: x: 4, y: 8, z: 12, core: 2. Of those that a mesh axis runs over, the one named last changes fastest.
Arguments:
- tokens: bfloat16 [98304, 2048], P(('ep', 'tp')), may hold values from -40 to 40
- norm_gain: float32 [2048], replicated, may hold values from 0.1 to 1.9
- routes: int32 [98304, 2], P(('ep', 'tp')), may hold values from 0 to 31, all different within a row; in each aligned block of 128 rows (0 to 127, 128 to 255, ...) at most 16 rows name the same one
- gates: float32 [98304, 2], P(('ep', 'tp')), may hold values from 0.25 to 2
- expert_gate: bfloat16 [32, 2048, 512], P('tp'), may hold values from -0.125 to 0.125
- expert_up: bfloat16 [32, 2048, 512], P('tp'), may hold values from -0.125 to 0.125
- expert_down: bfloat16 [32, 512, 2048], P('tp'), may hold values from -0.25 to 0.25
- shared_gate: bfloat16 [2048, 256], replicated, may hold values from -0.125 to 0.125
- shared_up: bfloat16 [2048, 256], replicated, may hold values from -0.125 to 0.125
- shared_down: bfloat16 [256, 2048], replicated, may hold values from -0.375 to 0.375
Outputs:
- mixed: bfloat16 [98304, 2048], P(('ep', 'tp'))
- load: float32 [32], replicated
Inputs may be any that keep to these rules, and one draw needn't show every extreme that they name: `routes`: each row names 2 different experts. Among the rows of one device no expert is named by more than 16 rows, and in every draw some expert is named by exactly 16 rows of some device.
All inputs are finite; a program needn't handle non-finite values.
Results may differ from a plain program's by a relative error of at most 0.002.
The roundings to bfloat16 on the way count: a program that leaves them out, or rounds other values in their place, can miss the bound.
Values may be sent and summed in bfloat16 or wider, within the bound.
A program may use at most 64 MiB of HBM per device.

v0:
```python
import jax
import jax.numpy as jnp
from jax import lax
from jax.sharding import Mesh
from jax.sharding import PartitionSpec as P

TP = ("tp_0", "tp_1")
EP = ("ep_0", "ep_1")
EP_TP = ("ep_0", "ep_1", "tp_0", "tp_1")


def by_axis(x, axes):
    for axis in axes:
        x = lax.psum(x, axis)
    return x


def layer_normed(token_block, norm_gain):
    values = token_block.astype(jnp.float32)
    center = jnp.mean(values, axis=-1, keepdims=True)
    spread = jnp.mean(jnp.square(values - center), axis=-1, keepdims=True)
    return ((values - center) * lax.rsqrt(spread + 1e-05) * norm_gain).astype(jnp.bfloat16)


def gated_mlp(row_block, w_gate, w_up, w_down):
    gate_part = jnp.dot(row_block, w_gate, preferred_element_type=jnp.float32)
    up_part = jnp.dot(row_block, w_up, preferred_element_type=jnp.float32)
    hidden = (jax.nn.silu(gate_part) * up_part).astype(jnp.bfloat16)
    return jnp.dot(hidden, w_down, preferred_element_type=jnp.float32)


def per_device(
    tokens,
    norm_gain,
    routes,
    gates,
    expert_gate,
    expert_up,
    expert_down,
    shared_gate,
    shared_up,
    shared_down,
):
    normed = layer_normed(tokens, norm_gain)
    count_rows, feature_count = normed.shape
    top_count = routes.shape[1]
    groups = lax.axis_size(TP)
    devices = lax.axis_size(EP) * groups
    capacity = 2 * count_rows * top_count // groups
    flat_expert = routes.reshape(-1)
    onehot = (flat_expert[:, None] == jnp.arange(groups, dtype=jnp.int32)[None, :]).astype(
        jnp.int32
    )
    earlier = jnp.cumsum(onehot, axis=0) - onehot
    slot_index = jnp.sum(earlier * onehot, axis=1)
    destination = flat_expert * capacity + slot_index
    local_counts = jnp.sum(onehot, axis=0).astype(jnp.float32)
    copies = jnp.repeat(normed, top_count, axis=0)
    outgoing = (
        jnp.zeros((groups * capacity, feature_count), jnp.bfloat16).at[destination].set(copies)
    )
    outgoing = outgoing.reshape(groups, capacity, feature_count)
    arrived = lax.all_to_all(outgoing, TP, split_axis=0, concat_axis=0, tiled=True)
    sources, slot_count, _ = arrived.shape
    result = gated_mlp(
        arrived.reshape(sources * slot_count, feature_count),
        expert_gate[0],
        expert_up[0],
        expert_down[0],
    )
    result = result.astype(jnp.bfloat16).reshape(sources, slot_count, feature_count)
    returned = lax.all_to_all(result, TP, split_axis=0, concat_axis=0, tiled=True)
    flat_returned = returned.reshape(groups * capacity, feature_count)
    per_copy = flat_returned[destination].reshape(count_rows, top_count, feature_count)
    routed = jnp.sum(gates[:, :, None] * per_copy.astype(jnp.float32), axis=1)
    shared_out = gated_mlp(normed, shared_gate, shared_up, shared_down)
    mixed = (routed + shared_out).astype(jnp.bfloat16)
    total_counts = by_axis(local_counts, EP_TP)
    load = total_counts * (groups / (count_rows * top_count * devices))
    return (mixed, load)


def solution(mesh):
    torus = Mesh(mesh.devices.reshape(12, 2, 8, 4), ("ep_0", "ep_1", "tp_0", "tp_1"))
    in_specs = (
        P(EP_TP, None),
        P(),
        P(EP_TP, None),
        P(EP_TP, None),
        P(TP, None, None),
        P(TP, None, None),
        P(TP, None, None),
        P(),
        P(),
        P(),
    )
    out_specs = (P(EP_TP, None), P())
    return jax.shard_map(
        per_device, mesh=torus, in_specs=in_specs, out_specs=out_specs, check_vma=False
    )
```

profile of v0, /device:TPU:704, one launch (start us, length us, event | category | flops | bytes accessed | tf_op | source)
XLA Modules:
  0.0 179.0 jit_solution(8228958169488088384)
XLA Ops:
  0.6 0.0 copy-start
  0.6 0.9 copy.15
  1.6 0.1 eq.29
  1.7 0.1 eq.25
  1.9 0.7 broadcast_multiply_fusion
  2.6 0.6 reduce-window.6
  3.1 0.2 slice_reduce_fusion
  3.4 0.1 copy.14
  3.5 0.1 mul.66
  3.6 1.2 convert_reduce_fusion
  4.8 1.3 fusion.15
  6.2 1.4 fusion.17
  7.6 1.6 broadcast_in_dim.5
  9.2 2.3 %reshape.101 = bf16[256,2048]{1,0:T(8,128)(2,1)} reshape(bf16[128,2,2048]{2,1,0:T(2,128)(2,1)} %broadcast_in_dim.5) | data formatting | bytes 2097152 | tf_op jit(solution)/shard_map/reshape | solution.py:58
  11.5 0.1 convert_reduce_fusion.1
  11.6 4.4 %scatter_custom_fusion = bf16[512,2048]{1,0:T(8,128)(2,1)} fusion(s32[256]{0:T(256)S(1)} %bitcast.43, bf16[256,2048]{1,0:T(8,128)(2,1)} %reshape.101, bf16[]{:T(256)} %constant.9.clone.1), kind=kCustom, calls=%fused_computation.22 | custom fusion | bytes 2097664 | tf_op jit(solution)/shard_map/scatter | solution.py:60
  16.1 0.0 copy-start.3
  16.1 60.6 %all_to_all.10 = bf16[32,16,2048]{2,1,0:T(8,128)(2,1)S(1)} all-to-all(bf16[32,16,2048]{2,1,0:T(8,128)(2,1)} %bitcast.39), channel_id=1, replica_groups=mesh['ep_0'=12,'ep_1'=2,'tp_0'=8,'tp_1'=4] {'tp_0','tp_1'}, dimensions={0} | all-to-all | bytes 4194304 | tf_op jit(solution)/shard_map/all_to_all | solution.py:63
  76.7 0.0 copy-start.1
  76.7 1.3 copy-done.1
  78.0 0.0 copy-done.3
  78.0 2.2 %fusion.4 = f32[512,512]{1,0:T(8,128)} fusion(bf16[512,2048]{1,0:T(8,128)(2,1)S(1)} %bitcast.41, bf16[1,2048,512]{2,1,0:T(8,128)(2,1)S(1)} %copy-done.3), kind=kOutput, calls=%fused_computation.8 | convolution fusion | flops 1073741824 | bytes 5242880 | tf_op jit(solution)/shard_map/dot_general | solution.py:26
  80.2 0.0 copy-done
  80.2 6.3 %convolution_convert_fusion = bf16[512,2048]{1,0:T(8,128)(2,1)} fusion(bf16[1,512,2048]{2,1,0:T(8,128)(2,1)S(1)} %copy-done, bf16[512,2048]{1,0:T(8,128)(2,1)} %bitcast.42, bf16[1,2048,512]{2,1,0:T(8,128)(2,1)} %param.15, f32[512,512]{1,0:T(8,128)} %fusion.4), kind=kOutput, calls=%fused_computation.2 | convolution fusion | flops 2150105088 | bytes 9437184 | tf_op jit(solution)/shard_map/dot_general | solution.py:29
  86.5 0.0 copy-start.2
  86.5 5.8 %all-to-all-start.1 = ((bf16[32,16,2048]{2,1,0:T(8,128)(2,1)}), bf16[32,16,2048]{2,1,0:T(8,128)(2,1)}, u32[]{:S(2)}, u32[]{:S(2)}) async-start(bf16[32,16,2048]{2,1,0:T(8,128)(2,1)} %bitcast.40), calls=%async_computation.1 | async-start | bytes 4194304 | tf_op jit(solution)/shard_map/all_to_all | solution.py:72
  92.3 0.0 copy-done.2
  92.3 0.1 copy.13
  92.4 20.4 %psum.28 = f32[32]{0:T(128)S(1)} all-reduce(f32[32]{0:T(128)S(1)} %convert_element_type.44), channel_id=1, replica_groups=mesh['ep_0'=12,'ep_1'=2,'tp_0'=8,'tp_1'=4] {'ep_0'}, use_global_device_ids=true, to_apply=%region_8.9 | all-reduce | flops 32 | bytes 256 | tf_op jit(solution)/shard_map/psum | solution.py:14
  112.8 2.5 %psum.29 = f32[32]{0:T(128)S(1)} all-reduce(f32[32]{0:T(128)S(1)} %psum.28), channel_id=1, replica_groups=mesh['ep_0'=12,'ep_1'=2,'tp_0'=8,'tp_1'=4] {'ep_1'}, use_global_device_ids=true, to_apply=%region_9.10 | all-reduce | flops 32 | bytes 256 | tf_op jit(solution)/shard_map/psum | solution.py:14
  115.3 33.4 %psum.30 = f32[32]{0:T(128)S(1)} all-reduce(f32[32]{0:T(128)S(1)} %psum.29), channel_id=1, replica_groups=mesh['ep_0'=12,'ep_1'=2,'tp_0'=8,'tp_1'=4] {'tp_0'}, use_global_device_ids=true, to_apply=%region_10.11 | all-reduce | flops 32 | bytes 256 | tf_op jit(solution)/shard_map/psum | solution.py:14
  148.6 10.6 %psum.31 = f32[32]{0:T(128)S(1)} all-reduce(f32[32]{0:T(128)S(1)} %psum.30), channel_id=1, replica_groups=mesh['ep_0'=12,'ep_1'=2,'tp_0'=8,'tp_1'=4] {'tp_1'}, use_global_device_ids=true, to_apply=%region_11.12 | all-reduce | flops 32 | bytes 256 | tf_op jit(solution)/shard_map/psum | solution.py:14
  159.2 0.5 broadcast_multiply_fusion.1
  159.7 1.5 fusion.34
  161.3 0.0 all-to-all-done.1
  161.3 5.2 %gather_fusion = bf16[256,2048]{1,0:T(8,128)(2,1)} fusion(bf16[512,2048]{1,0:T(8,128)(2,1)} %bitcast.9, s32[1024]{0:T(1024)S(1)} %pad_clamp_fusion), kind=kCustom, calls=%fused_computation | custom fusion | bytes 2098176 | tf_op jit(solution)/shard_map/gather | solution.py:74
  166.5 3.4 %reshape.88 = f32[128,2,2048]{2,1,0:T(2,128)} reshape(bf16[256,2048]{1,0:T(8,128)(2,1)} %gather_fusion) | data formatting | bytes 3145728 | tf_op jit(solution)/shard_map/convert_element_type | solution.py:75
  169.9 5.7 %multiply_reduce_fusion = f32[128,2048]{1,0:T(8,128)} fusion(f32[128,2,2048]{2,1,0:T(2,128)} %reshape.88, f32[128,2]{1,0:T(8,128)S(1)} %copy.13), kind=kLoop, calls=%fused_computation.10 | loop fusion | flops 786432 | bytes 3146752 | tf_op jit(solution)/shard_map/reduce_sum | solution.py:75
  175.6 3.4 %fusion = bf16[128,2048]{1,0:T(8,128)(2,1)} fusion(f32[128,2048]{1,0:T(8,128)} %multiply_reduce_fusion, bf16[256,2048]{1,0:T(8,128)(2,1)} %param.19, bf16[128,2048]{1,0:T(8,128)(2,1)S(1)} %fusion.17, bf16[2048,256]{1,0:T(8,128)(2,1)} %param.18, f32[128,256]{1,0:T(8,128)S(1)} %fusion.34), kind=kOutput, calls=%fused_computation.4 | convolution fusion | flops 269156352 | bytes 4325376 | tf_op jit(solution)/shard_map/dot_general | solution.py:29
  (8 shorter events, 0.1 us)
Async XLA Ops:
  0.6 79.6 %copy-start = (bf16[1,512,2048]{2,1,0:T(8,128)(2,1)S(1)}, bf16[1,512,2048]{2,1,0:T(8,128)(2,1)}, u32[]{:S(2)}) copy-start(bf16[1,512,2048]{2,1,0:T(8,128)(2,1)} %param.16) | copy-start | bytes 6291460
  16.1 61.9 %copy-start.3 = (bf16[1,2048,512]{2,1,0:T(8,128)(2,1)S(1)}, bf16[1,2048,512]{2,1,0:T(8,128)(2,1)}, u32[]{:S(2)}) copy-start(bf16[1,2048,512]{2,1,0:T(8,128)(2,1)} %param.14) | copy-start | bytes 6291460
  76.7 1.3 copy-start.1
  86.5 5.9 %copy-start.2 = (f32[128,2]{0,1:T(2,128)S(1)}, f32[128,2]{0,1:T(2,128)}, u32[]{:S(2)}) copy-start(f32[128,2]{0,1:T(2,128)} %param.13) | copy-start | bytes 3076
  86.5 74.8 %all-to-all-start.1 = ((bf16[32,16,2048]{2,1,0:T(8,128)(2,1)}), bf16[32,16,2048]{2,1,0:T(8,128)(2,1)}, u32[]{:S(2)}, u32[]{:S(2)}) async-start(bf16[32,16,2048]{2,1,0:T(8,128)(2,1)} %bitcast.40), calls=%async_computation.1 | async-start | bytes 4194304 | tf_op jit(solution)/shard_map/all_to_all | solution.py:72
where the time goes:
time: 180 us; the launch traced here: 179 us
  blocking collectives  127 us (71%)
  local copies, waits for them, and re-layouts  20 us (11%)
  matrix products  13.5 us (8%)
  other arithmetic  11.7 us (6%)
  starting transfers between devices  5.84 us (3%)
    psum x4, blocking collectives, by_axis(): x = lax.psum(x, axis)  66.8 us
    all_to_all x1, blocking collectives, per_device(): lax.all_to_all(outgoing, TP, split_axis=0, concat_axis=0, tiled=True)  60.6 us
    dot_general x2, matrix products, gated_mlp(): return jnp.dot(hidden, w_down, preferred_element_type=jnp.float32)  9.7 us
    all_to_all x1, starting transfers between devices, per_device(): lax.all_to_all(result, TP, split_axis=0, concat_axis=0, tiled=True)  5.84 us
    reduce_sum x1, other arithmetic, per_device(): routed = jnp.sum(gates[:, :, None] * per_copy.astype(jnp.float32), axis=1)  5.72 us
    gather x1, local copies, waits for them, and re-layouts, per_device(): flat_returned[destination].reshape(count_rows, top_count, feature_count)  5.2 us
    scatter x1, local copies, waits for them, and re-layouts, per_device(): jnp.zeros((groups * capacity, feature_count), jnp.bfloat16).at[destination]  4.43 us
    dot_general x2, matrix products, gated_mlp(): gate_part = jnp.dot(row_block, w_gate, preferred_element_type=jnp.float32)  3.75 us
  transfers between devices with their start and end apart: 1, of which 0 were waited for; matrix products, arithmetic and copies ran while one was open for 1% of the time, Pallas kernels for 0%

commit v1 on v0

v1 whole, which is shorter than its diff:
```python
import functools

import jax
import jax.numpy as jnp
from jax import lax
from jax.experimental import pallas as pl
from jax.experimental.pallas import tpu as pltpu
from jax.sharding import PartitionSpec as P

NY, NX, NZ = 8, 4, 12
CAP = 16
MESH = pl.DeviceIdType.MESH
F32, BF16 = jnp.float32, jnp.bfloat16

SLOTS = [(dy, dx) for dx in (0, 1, 3, 2) for dy in (0, 4, 3, 5, 2, 6, 1, 7)]
GROUP = 8
ROWS = GROUP * CAP
GROUPS = len(SLOTS) // GROUP


def kernel(
    routes_ref,
    gates_ref,
    gain_ref,
    tokens_hbm,
    wg_hbm,
    wu_hbm,
    wd_hbm,
    sg_hbm,
    su_hbm,
    sd_hbm,
    mixed_ref,
    load_ref,
    tok,
    normed,
    wg,
    wu,
    wd,
    sg,
    su,
    sd,
    outgoing,
    arrived,
    result,
    returned,
    hidden,
    shidden,
    acc,
    csrc,
    cdst,
    local_sem,
    send_sem,
    recv_sem,
    back_send,
    back_recv,
    csend,
    crecv,
):
    ep, tp = lax.axis_index("ep"), lax.axis_index("tp")
    my_y, my_x = tp // NX, tp % NX
    my_z, my_c = ep // 2, ep % 2

    def plane(dy, dx):
        return {"tp": ((my_y + dy) % NY) * NX + (my_x + dx) % NX}

    def along_z(dz):
        return {"ep": ((my_z + dz) % NZ) * 2 + my_c}

    partner = {"ep": my_z * 2 + 1 - my_c}

    copies = [
        pltpu.make_async_copy(src, dst, local_sem.at[i])
        for i, (src, dst) in enumerate(
            [
                (tokens_hbm, tok),
                (sg_hbm, sg),
                (su_hbm, su),
                (sd_hbm, sd),
                (wg_hbm.at[0], wg),
                (wu_hbm.at[0], wu),
                (wd_hbm.at[0], wd),
            ]
        )
    ]
    for c in copies:
        c.start()

    peers = (
        [plane(dy, dx) for dy, dx in SLOTS if (dy, dx) != (0, 0)]
        + [along_z(dz) for dz in range(1, NZ)]
        + [partner]
    )
    barrier = pltpu.get_barrier_semaphore()
    for peer in peers:
        pl.semaphore_signal(barrier, inc=1, device_id=peer, device_id_type=MESH)

    routes = routes_ref[...]
    lane = lax.broadcasted_iota(jnp.int32, (1, 128), 1)
    lane_expert = jnp.full((1, 128), -1, jnp.int32)
    for j, (dy, dx) in enumerate(SLOTS):
        expert = ((my_y + dy) % NY) * NX + (my_x + dx) % NX
        lane_expert = jnp.where(lane == j, expert, lane_expert)
    ti = lax.broadcasted_iota(jnp.int32, (128, 128), 0)
    tj = lax.broadcasted_iota(jnp.int32, (128, 128), 1)
    hot = [(routes[:, k : k + 1] == lane_expert).astype(F32) for k in range(2)]
    both = (hot[0] + hot[1]).astype(BF16)
    earlier = jnp.dot((tj < ti).astype(F32).astype(BF16), both, preferred_element_type=F32)
    at = earlier + (CAP * lane).astype(F32)
    pos = [jnp.sum(h * at, axis=1, keepdims=True).astype(jnp.int32) for h in hot]
    pos_row = [
        jnp.sum(jnp.where(ti == tj, p, 0), axis=0, keepdims=True) for p in pos
    ]
    absolute = [(routes[:, k : k + 1] == lane).astype(F32) for k in range(2)]
    counts = jnp.sum(absolute[0] + absolute[1], axis=0, keepdims=True)
    csrc[0] = jnp.broadcast_to(counts, (8, 128))

    copies[0].wait()
    gain = gain_ref[...]

    def norm(i, carry):
        rows = pl.ds(pl.multiple_of(i * 16, 16), 16)
        values = tok[rows, :].astype(F32)
        values = values - jnp.mean(values, axis=-1, keepdims=True)
        spread = jnp.mean(values * values, axis=-1, keepdims=True)
        normed[rows, :] = (values * lax.rsqrt(spread + 1e-05) * gain).astype(BF16)
        return carry

    lax.fori_loop(0, 8, norm, 0)

    def build(g):
        rows = slice(g * ROWS, (g + 1) * ROWS)
        pick = jnp.where((ti + g * ROWS == pos_row[0]) | (ti + g * ROWS == pos_row[1]), 1.0, 0.0)
        pick = pick.astype(BF16)
        for n in range(4):
            cols = slice(n * 512, (n + 1) * 512)
            outgoing[rows, cols] = jnp.dot(
                pick, normed[:, cols], preferred_element_type=F32
            ).astype(BF16)

    def dispatch(j):
        rows = pl.ds(j * CAP, CAP)
        return pltpu.make_async_remote_copy(
            src_ref=outgoing.at[rows],
            dst_ref=arrived.at[rows],
            send_sem=send_sem.at[j],
            recv_sem=recv_sem.at[j],
            device_id=plane(*SLOTS[j]),
            device_id_type=MESH,
        )

    def give_back(j):
        rows = pl.ds(j * CAP, CAP)
        dy, dx = SLOTS[j]
        return pltpu.make_async_remote_copy(
            src_ref=result.at[rows],
            dst_ref=returned.at[rows],
            send_sem=back_send.at[j],
            recv_sem=back_recv.at[j],
            device_id=plane(-dy, -dx),
            device_id_type=MESH,
        )

    def in_group(g):
        return [j for j in range(g * GROUP, (g + 1) * GROUP) if j != 0]

    stages = (
        [plane(0, d) for d in range(1, NX)],
        [plane(d, 0) for d in range(1, NY)],
        [along_z(d) for d in range(1, NZ)],
        [partner],
    )
    starts = [sum(len(s) for s in stages[:i]) for i in range(len(stages))]

    def count_copy(stage, i):
        n = starts[stage] + i
        return pltpu.make_async_remote_copy(
            src_ref=csrc.at[stage],
            dst_ref=cdst.at[n],
            send_sem=csend.at[n],
            recv_sem=crecv.at[n],
            device_id=stages[stage][i],
            device_id_type=MESH,
        )

    def count_send(stage):
        for i in range(len(stages[stage])):
            count_copy(stage, i).start()

    def count_sum(stage):
        total = csrc[stage]
        for i in range(len(stages[stage])):
            count_copy(stage, i).wait_recv()
            total = total + cdst[starts[stage] + i]
        return total

    build(0)
    arrived[0:CAP, :] = outgoing[0:CAP, :]
    pl.semaphore_wait(barrier, len(peers))
    for g in range(GROUPS):
        if g + 1 < GROUPS:
            build(g + 1)
        for j in in_group(g):
            dispatch(j).start()
    count_send(0)

    for c in copies[1:4]:
        c.wait()
    gate = jnp.dot(normed[...], sg[...], preferred_element_type=F32)
    up = jnp.dot(normed[...], su[...], preferred_element_type=F32)
    shidden[...] = (gate / (1.0 + jnp.exp(-gate)) * up).astype(BF16)
    for n in range(4):
        cols = slice(n * 512, (n + 1) * 512)
        acc[:, cols] = jnp.dot(shidden[...], sd[:, cols], preferred_element_type=F32)

    csrc[1] = count_sum(0)
    count_send(1)

    for c in copies[4:]:
        c.wait()
    for g in range(GROUPS):
        rows = slice(g * ROWS, (g + 1) * ROWS)
        for j in in_group(g):
            dispatch(j).wait_recv()
        for n in range(2):
            cols = slice(n * 256, (n + 1) * 256)
            gate = jnp.dot(arrived[rows, :], wg[:, cols], preferred_element_type=F32)
            up = jnp.dot(arrived[rows, :], wu[:, cols], preferred_element_type=F32)
            hidden[:, cols] = (gate / (1.0 + jnp.exp(-gate)) * up).astype(BF16)
        for n in range(4):
            cols = slice(n * 512, (n + 1) * 512)
            result[rows, cols] = jnp.dot(
                hidden[...], wd[:, cols], preferred_element_type=F32
            ).astype(BF16)
        if g == 0:
            returned[0:CAP, :] = result[0:CAP, :]
        for j in in_group(g):
            give_back(j).start()
        if g == 1:
            csrc[2] = count_sum(1)
            count_send(2)
        if g == 3:
            csrc[3] = count_sum(2)
            count_send(3)

    weight = [gates_ref[:, k : k + 1] for k in range(2)]
    for g in range(GROUPS):
        rows = slice(g * ROWS, (g + 1) * ROWS)
        pick = jnp.concatenate(
            [jnp.where(tj + g * ROWS == p, 1.0, 0.0).astype(BF16) for p in pos], axis=0
        )
        for j in in_group(g):
            give_back(j).wait_recv()
        for n in range(4):
            cols = slice(n * 512, (n + 1) * 512)
            pair = jnp.dot(pick, returned[rows, cols], preferred_element_type=F32)
            total = acc[:, cols] + (weight[0] * pair[:128] + weight[1] * pair[128:])
            if g + 1 < GROUPS:
                acc[:, cols] = total
            else:
                mixed_ref[:, cols] = total.astype(BF16)

    load_ref[...] = count_sum(3) * (32 / 196608)
    for j in range(1, len(SLOTS)):
        dispatch(j).wait_send()
        give_back(j).wait_send()
    for stage in range(4):
        for i in range(len(stages[stage])):
            count_copy(stage, i).wait_send()


def per_device(tokens, norm_gain, routes, gates, wg, wu, wd, sg, su, sd):
    vmem = pl.BlockSpec(memory_space=pltpu.VMEM)
    anywhere = pl.BlockSpec(memory_space=pl.ANY)
    dma = pltpu.SemaphoreType.DMA
    slots = len(SLOTS)
    total = slots * CAP
    ncount = NX - 1 + NY - 1 + NZ - 1 + 1
    mixed, load = pl.pallas_call(
        kernel,
        out_shape=(
            jax.ShapeDtypeStruct((128, 2048), BF16),
            jax.ShapeDtypeStruct((8, 128), F32),
        ),
        in_specs=[vmem] * 3 + [anywhere] * 7,
        out_specs=(vmem, vmem),
        scratch_shapes=[
            pltpu.VMEM((128, 2048), BF16),
            pltpu.VMEM((128, 2048), BF16),
            pltpu.VMEM((2048, 512), BF16),
            pltpu.VMEM((2048, 512), BF16),
            pltpu.VMEM((512, 2048), BF16),
            pltpu.VMEM((2048, 256), BF16),
            pltpu.VMEM((2048, 256), BF16),
            pltpu.VMEM((256, 2048), BF16),
            pltpu.VMEM((total, 2048), BF16),
            pltpu.VMEM((total, 2048), BF16),
            pltpu.VMEM((total, 2048), BF16),
            pltpu.VMEM((total, 2048), BF16),
            pltpu.VMEM((ROWS, 512), BF16),
            pltpu.VMEM((128, 256), BF16),
            pltpu.VMEM((128, 2048), F32),
            pltpu.VMEM((4, 8, 128), F32),
            pltpu.VMEM((ncount, 8, 128), F32),
            dma((7,)),
            dma((slots,)),
            dma((slots,)),
            dma((slots,)),
            dma((slots,)),
            dma((ncount,)),
            dma((ncount,)),
        ],
        compiler_params=pltpu.CompilerParams(
            collective_id=0, has_side_effects=True, vmem_limit_bytes=56 << 20
        ),
    )(routes, gates, norm_gain.reshape(1, -1), tokens, wg, wu, wd, sg, su, sd)
    return mixed, load[0, :32]


def solution(mesh):
    rows = P(("ep", "tp"), None)
    expert = P("tp", None, None)
    return jax.shard_map(
        per_device,
        mesh=mesh,
        in_specs=(rows, P(), rows, rows, expert, expert, expert, P(), P(), P()),
        out_specs=(rows, P()),
        check_vma=False,
    )
```

time: 180 us -> 123 us (0.68)
  the two profiles are of different devices: /device:TPU:704 before, /device:TPU:1 now
where the time goes in v1:
time: 123 us; the launch traced here: 122 us
  Pallas kernels  116 us (94%)
  local copies, waits for them, and re-layouts  5.9 us (5%)
    pallas_call x1, Pallas kernels, per_device(): pl.pallas_call(kernel, out_shape=(jax.ShapeDtypeStruct((128, 2048), BF16)...  116 us
    unnamed x3, local copies, waits for them, and re-layouts  4.71 us

profile of v1, /device:TPU:1, one launch (start us, length us, event | category | flops | bytes accessed | tf_op | source)
XLA Modules:
  0.0 122.2 jit_solution(943684463861883319)
XLA Ops:
  0.6 1.4 %copy.12.routes_ref = s32[128,2]{1,0:T(8,128)} copy(s32[128,2]{0,1:T(2,128)} %param.12) | data formatting | bytes 2048 | tf_op args[2]
  2.0 1.4 %copy.13.gates_ref = f32[128,2]{1,0:T(8,128)} copy(f32[128,2]{0,1:T(2,128)} %param.13) | data formatting | bytes 2048 | tf_op args[3]
  3.5 115.7 %shard_map.113 = (bf16[128,2048]{1,0:T(8,128)(2,1)}, f32[8,128]{1,0:T(8,128)}) custom-call(s32[128,2]{1,0:T(8,128)} %copy.12.routes_ref, f32[128,2]{1,0:T(8,128)} %copy.13.gates_ref, f32[1,2048]{1,0:T(1,128)} %bitcast.3, bf16[128,2048]{1,0:T(8,128)(2,1)} %tokens_hbm.1, bf16[1,2048,512]{2,1,0:T(8,128)(2,1)} %wg_hbm.1, bf16[1,2048,512]{2,1,0:T(8,128)(2,1)} %wu_hbm.1, ...), custom_call_target="tpu_custom_call" | custom-call | tf_op jit(solution)/shard_map/pallas_call | solution.py:278
  119.2 1.2 slice_bitcast_fusion
  120.3 1.9 %copy.15 = bf16[128,2048]{1,0:T(8,128)(2,1)} copy(bf16[128,2048]{1,0:T(8,128)(2,1)} %get-tuple-element.8) | data formatting | bytes 1048576

commit v2 on v1

v2 whole, which is shorter than its diff:
```python
import jax
import jax.numpy as jnp
from jax import lax
from jax.experimental import pallas as pl
from jax.experimental.pallas import tpu as pltpu
from jax.sharding import PartitionSpec as P

NY, NX, NZ = 8, 4, 12
CAP = 16
MESH = pl.DeviceIdType.MESH
F32, BF16 = jnp.float32, jnp.bfloat16

SHIFTS = (-2, 2, -1, 1, 0)
FIRST_B = 2
TO_A = len(SHIFTS) * NX
SLOTS = TO_A + (len(SHIFTS) - FIRST_B) * NX
GROUP = 2 * NX
ROWS = GROUP * CAP
SELF_A, SELF_B = TO_A - NX, SLOTS - NX
SUBS = 4
SUB = 512 // SUBS


def kernel(
    routes_ref,
    gates_ref,
    gain_ref,
    tokens_hbm,
    wg_hbm,
    wu_hbm,
    wd_hbm,
    sg_hbm,
    su_hbm,
    sd_hbm,
    mixed_ref,
    load_ref,
    tok,
    normed,
    weights,
    stage,
    sg,
    su,
    sd,
    outgoing,
    arrived,
    result,
    returned,
    hidden,
    shidden,
    acc,
    csrc,
    cdst,
    local_sem,
    weight_sem,
    stage_sem,
    send_sem,
    recv_sem,
    back_send,
    back_recv,
    csend,
    crecv,
    ysend,
    yrecv,
    zsend,
    zrecv,
    ready,
):
    ep, tp = lax.axis_index("ep"), lax.axis_index("tp")
    my_y, my_x = tp // NX, tp % NX
    my_z, core = ep // 2, ep % 2

    def device(dy=0, dx=0, dz=0, on=None):
        return {
            "ep": lax.rem(my_z + dz + NZ, NZ) * 2 + (core if on is None else on),
            "tp": lax.rem(my_y + dy + NY, NY) * NX + lax.rem(my_x + dx + NX, NX),
        }

    def remote(src, dst, send, recv, to):
        return pltpu.make_async_remote_copy(
            src_ref=src, dst_ref=dst, send_sem=send, recv_sem=recv, device_id=to, device_id_type=MESH
        )

    def signal(sem, to):
        pl.semaphore_signal(sem, inc=1, device_id=to, device_id_type=MESH)

    barrier = pltpu.get_barrier_semaphore()
    peers = (
        [device(dy, dx) for dy in range(-2, 3) for dx in range(NX) if (dy, dx) != (0, 0)]
        + [device(dy=d) for d in (3, 4, 5)]
        + [device(dz=d) for d in range(1, NZ)]
    )
    for peer in peers:
        signal(barrier, peer)

    copies = [
        pltpu.make_async_copy(src, dst, local_sem.at[i])
        for i, (src, dst) in enumerate(
            [(tokens_hbm, tok), (sg_hbm, sg), (su_hbm, su), (sd_hbm, sd)]
        )
    ]
    copies[0].start()

    def block_of(k):
        at = pl.ds(k % 4 * 512, 512)
        return (wg_hbm.at[0, at, :], wu_hbm.at[0, at, :], wd_hbm.at[0, :, at])[k // 4]

    own = [
        pltpu.make_async_copy(block_of(k), weights.at[k], weight_sem.at[k]) for k in range(12)
    ]
    third = lax.rem(my_z, 4) * 512
    third = pl.multiple_of(third, 512)
    staged = [
        pltpu.make_async_copy(src, stage, stage_sem)
        for src in (
            wg_hbm.at[0, pl.ds(third, 512), :],
            wu_hbm.at[0, pl.ds(third, 512), :],
            wd_hbm.at[0, :, pl.ds(third, 512)],
        )
    ]

    def sub(ref, piece, q):
        return ref.at[piece, pl.ds(q * SUB, SUB), :]

    def across(q):
        return remote(
            stage.at[pl.ds(q * SUB, SUB), :],
            sub(weights, my_z, q),
            ysend.at[q],
            yrecv.at[q],
            device(dy=4),
        )

    def round_z(way, step, q):
        sign = 1 - 2 * way
        piece = lax.rem(my_z - sign * (step - 1) + NZ, NZ)
        return remote(
            sub(weights, piece, q),
            sub(weights, piece, q),
            zsend.at[way, step - 1, q],
            zrecv.at[way, step - 1, q],
            device(dz=sign),
        )

    def goes(way, step, q):
        return step < 6 or (step == 6 and (q < SUBS // 2) == (way == 0))

    @pl.when(core == 1)
    def _():
        for part in range(3):

            @pl.when(my_z // 4 == part)
            def _():
                staged[part].start()

        pl.semaphore_wait(barrier, len(peers))
        signal(barrier, device(on=0))
        staged[0].wait()
        for q in range(SUBS):
            across(q).start()

    @pl.when(core == 0)
    def _():
        for c in own:
            c.start()

    for c in copies[1:]:
        c.start()

    shape = (SLOTS, 128)
    slot = lax.broadcasted_iota(jnp.int32, shape, 0)
    to_b = slot >= TO_A
    index = jnp.where(to_b, slot - TO_A + FIRST_B * NX, slot)
    shift = jnp.zeros(shape, jnp.int32)
    for g, dy in enumerate(SHIFTS):
        shift = jnp.where(index // NX == g, dy + NY, shift)
    shift = jnp.where(to_b, shift + NY // 2, shift)
    expert = (my_y + shift) % NY * NX + (my_x + index % NX) % NX
    routes = [routes_ref[k : k + 1, :] for k in range(2)]
    hot = [(r == expert).astype(F32) for r in routes]
    ti = lax.broadcasted_iota(jnp.int32, (128, 128), 0)
    tj = lax.broadcasted_iota(jnp.int32, (128, 128), 1)
    earlier = jnp.dot(
        (hot[0] + hot[1]).astype(BF16),
        (ti < tj).astype(F32).astype(BF16),
        preferred_element_type=F32,
    )
    at = earlier + (CAP * slot).astype(F32)
    pos_row = [jnp.sum(h * at, axis=0, keepdims=True).astype(jnp.int32) for h in hot]
    pos = [jnp.sum(jnp.where(ti == tj, p, 0), axis=1, keepdims=True) for p in pos_row]
    weight = [
        jnp.sum(jnp.where(ti == tj, gates_ref[k : k + 1, :], 0.0), axis=1, keepdims=True)
        for k in range(2)
    ]
    route_col = [jnp.sum(jnp.where(ti == tj, r, 0), axis=1, keepdims=True) for r in routes]
    counts = jnp.sum(
        (route_col[0] == tj).astype(F32) + (route_col[1] == tj).astype(F32), axis=0, keepdims=True
    )
    csrc[0] = jnp.broadcast_to(counts, (8, 128))

    copies[0].wait()
    gain = gain_ref[...]

    def norm(i, carry):
        rows = pl.ds(pl.multiple_of(i * 16, 16), 16)
        values = tok[rows, :].astype(F32)
        values = values - jnp.mean(values, axis=-1, keepdims=True)
        spread = jnp.mean(values * values, axis=-1, keepdims=True)
        normed[rows, :] = (values * lax.rsqrt(spread + 1e-05) * gain).astype(BF16)
        return carry

    lax.fori_loop(0, 8, norm, 0)

    def build(b):
        rows = slice(b * 128, (b + 1) * 128)
        pick = (ti + b * 128 == pos_row[0]) | (ti + b * 128 == pos_row[1])
        pick = jnp.where(pick, 1.0, 0.0).astype(BF16)
        for n in range(4):
            cols = slice(n * 512, (n + 1) * 512)
            outgoing[rows, cols] = jnp.dot(
                pick, normed[:, cols], preferred_element_type=F32
            ).astype(BF16)

    def rows_of(j):
        return pl.ds(pl.multiple_of(j * CAP, CAP), CAP)

    def dispatch(host, g, dx):
        j = g * NX + dx + (SLOTS - TO_A) * host
        r = g * GROUP + 2 * dx + core
        return remote(
            outgoing.at[rows_of(j)],
            arrived.at[rows_of(r)],
            send_sem.at[j],
            recv_sem.at[r],
            device(SHIFTS[g], dx, on=host),
        )

    last = len(SHIFTS) - 1
    to_partner = dispatch(1 - core, last, 0)
    self_j = SELF_A + (SELF_B - SELF_A) * core
    self_r = last * GROUP + core

    def arrival(g, dx, c):
        r = g * GROUP + 2 * dx + c
        return remote(
            outgoing.at[rows_of(0)], arrived.at[rows_of(r)], send_sem.at[0], recv_sem.at[r], device(dy=1)
        )

    def give_back(g, dx, c):
        r = g * GROUP + 2 * dx + c
        j = g * NX + dx + (SLOTS - TO_A) * core
        return remote(
            result.at[rows_of(r)],
            returned.at[rows_of(j)],
            back_send.at[r],
            back_recv.at[j],
            device(-SHIFTS[g], -dx, on=c),
        )

    def got_back(j):
        return remote(
            result.at[rows_of(0)], returned.at[rows_of(j)], back_send.at[0], back_recv.at[j], device(dy=1)
        )

    stages = (
        [device(dx=d) for d in range(1, NX)],
        [device(dy=d) for d in range(1, NY)],
        [device(dz=d) for d in range(1, NZ)],
        [device(on=1 - core)],
    )
    starts = [sum(len(s) for s in stages[:i]) for i in range(len(stages))]

    def count_copy(stage_at, i):
        n = starts[stage_at] + i
        return remote(csrc.at[stage_at], cdst.at[n], csend.at[n], crecv.at[n], stages[stage_at][i])

    def count_send(stage_at):
        for i in range(len(stages[stage_at])):
            count_copy(stage_at, i).start()

    def count_sum(stage_at):
        total = csrc[stage_at]
        for i in range(len(stages[stage_at])):
            count_copy(stage_at, i).wait_recv()
            total = total + cdst[starts[stage_at] + i]
        return total

    def send_block(b):
        for j in range(b * 8, (b + 1) * 8):
            if j in (SELF_A, SELF_B):
                continue
            host = int(j >= TO_A)
            i = j - (SLOTS - TO_A) * host
            dispatch(host, i // NX, i % NX).start()

    build(0)

    @pl.when(core == 0)
    def _():
        pl.semaphore_wait(barrier, len(peers) + 1)
        signal(ready, device(on=1))

    @pl.when(core == 1)
    def _():
        pl.semaphore_wait(ready, 1)

    for b in range(SLOTS // 8):
        if b + 1 < SLOTS // 8:
            build(b + 1)
        send_block(b)
    arrived[rows_of(self_r), :] = outgoing[rows_of(self_j), :]
    to_partner.start()
    count_send(0)

    for c in copies[1:]:
        c.wait()
    gate = jnp.dot(normed[...], sg[...], preferred_element_type=F32)
    up = jnp.dot(normed[...], su[...], preferred_element_type=F32)
    shidden[...] = (gate / (1.0 + jnp.exp(-gate)) * up).astype(BF16)
    for n in range(4):
        cols = slice(n * 512, (n + 1) * 512)
        acc[:, cols] = jnp.dot(shidden[...], sd[:, cols], preferred_element_type=F32)

    csrc[1] = count_sum(0)
    count_send(1)

    def serve(g):
        rows = slice(g * ROWS, (g + 1) * ROWS)
        pairs = [(dx, c) for dx in range(NX) for c in range(2) if (g, dx) != (last, 0)]
        for dx, c in pairs:
            arrival(g, dx, c).wait_recv()
        if g == last:
            arrival(g, 0, 1 - core).wait_recv()
        for n in range(2):
            cols = slice(n * 256, (n + 1) * 256)
            gate = jnp.zeros((ROWS, 256), F32)
            up = jnp.zeros((ROWS, 256), F32)
            for k in range(4):
                x = arrived[rows, k * 512 : (k + 1) * 512]
                gate = gate + jnp.dot(x, weights[k, :, cols], preferred_element_type=F32)
                up = up + jnp.dot(x, weights[4 + k, :, cols], preferred_element_type=F32)
            hidden[:, cols] = (gate / (1.0 + jnp.exp(-gate)) * up).astype(BF16)
        for n in range(4):
            cols = slice(n * 512, (n + 1) * 512)
            result[rows, cols] = jnp.dot(
                hidden[...], weights[8 + n], preferred_element_type=F32
            ).astype(BF16)
        for dx, c in pairs:
            give_back(g, dx, c).start()
        if g == last:
            give_back(g, 0, 1 - core).start()
            returned[rows_of(self_j), :] = result[rows_of(self_r), :]

    @pl.when(core == 0)
    def _():
        for c in own:
            c.wait()
        for g in range(FIRST_B):
            serve(g)

    @pl.when(core == 1)
    def _():
        for q in range(SUBS):
            across(q).wait_recv()
            for way in range(2):
                round_z(way, 1, q).start()
        for step in range(1, 7):
            for q in range(SUBS):
                for way in range(2):
                    if goes(way, step, q):
                        round_z(way, step, q).wait_recv()
                        if goes(way, step + 1, q):
                            round_z(way, step + 1, q).start()

    csrc[2] = count_sum(1)
    count_send(2)
    for g in range(FIRST_B, len(SHIFTS)):
        serve(g)
    csrc[3] = count_sum(2)
    count_send(3)

    for b in range(SLOTS // 8):
        rows = slice(b * 128, (b + 1) * 128)
        pick = jnp.concatenate(
            [jnp.where(tj + b * 128 == p, 1.0, 0.0).astype(BF16) for p in pos], axis=0
        )
        for j in range(b * 8, (b + 1) * 8):
            if j not in (SELF_A, SELF_B):
                got_back(j).wait_recv()
            else:

                @pl.when(core == int(j == SELF_A))
                def _():
                    got_back(j).wait_recv()

        for n in range(4):
            cols = slice(n * 512, (n + 1) * 512)
            pair = jnp.dot(pick, returned[rows, cols], preferred_element_type=F32)
            total = acc[:, cols] + (weight[0] * pair[:128] + weight[1] * pair[128:])
            if b + 1 < SLOTS // 8:
                acc[:, cols] = total
            else:
                mixed_ref[:, cols] = total.astype(BF16)

    load_ref[...] = count_sum(3)[0:1, 0:32] * (32 / 196608)

    for j in range(SLOTS):
        if j not in (SELF_A, SELF_B):
            host = int(j >= TO_A)
            i = j - (SLOTS - TO_A) * host
            dispatch(host, i // NX, i % NX).wait_send()
    to_partner.wait_send()

    def sent_back(g):
        for dx in range(NX):
            for c in range(2):
                if (g, dx) != (last, 0):
                    give_back(g, dx, c).wait_send()
        if g == last:
            give_back(g, 0, 1 - core).wait_send()

    for g in range(FIRST_B, len(SHIFTS)):
        sent_back(g)

    @pl.when(core == 0)
    def _():
        for g in range(FIRST_B):
            sent_back(g)

    @pl.when(core == 1)
    def _():
        for q in range(SUBS):
            across(q).wait_send()
        for step in range(1, 7):
            for q in range(SUBS):
                for way in range(2):
                    if goes(way, step, q):
                        round_z(way, step, q).wait_send()

    for stage_at in range(4):
        for i in range(len(stages[stage_at])):
            count_copy(stage_at, i).wait_send()


def per_device(tokens, norm_gain, routes, gates, wg, wu, wd, sg, su, sd):
    vmem = pl.BlockSpec(memory_space=pltpu.VMEM)
    anywhere = pl.BlockSpec(memory_space=pl.ANY)
    dma = pltpu.SemaphoreType.DMA
    landed = len(SHIFTS) * GROUP
    ncount = NX - 1 + NY - 1 + NZ - 1 + 1
    mixed, load = pl.pallas_call(
        kernel,
        out_shape=(
            jax.ShapeDtypeStruct((128, 2048), BF16),
            jax.ShapeDtypeStruct((1, 32), F32),
        ),
        in_specs=[vmem] * 3 + [anywhere] * 7,
        out_specs=(vmem, vmem),
        scratch_shapes=[
            pltpu.VMEM((128, 2048), BF16),
            pltpu.VMEM((128, 2048), BF16),
            pltpu.VMEM((12, 512, 512), BF16),
            pltpu.VMEM((512, 512), BF16),
            pltpu.VMEM((2048, 256), BF16),
            pltpu.VMEM((2048, 256), BF16),
            pltpu.VMEM((256, 2048), BF16),
            pltpu.VMEM((SLOTS * CAP, 2048), BF16),
            pltpu.VMEM((landed * CAP, 2048), BF16),
            pltpu.VMEM((landed * CAP, 2048), BF16),
            pltpu.VMEM((SLOTS * CAP, 2048), BF16),
            pltpu.VMEM((ROWS, 512), BF16),
            pltpu.VMEM((128, 256), BF16),
            pltpu.VMEM((128, 2048), F32),
            pltpu.VMEM((4, 8, 128), F32),
            pltpu.VMEM((ncount, 8, 128), F32),
            dma((4,)),
            dma((12,)),
            dma(()),
            dma((SLOTS,)),
            dma((landed,)),
            dma((landed,)),
            dma((SLOTS,)),
            dma((ncount,)),
            dma((ncount,)),
            dma((SUBS,)),
            dma((SUBS,)),
            dma((2, 6, SUBS)),
            dma((2, 6, SUBS)),
            pltpu.SemaphoreType.REGULAR,
        ],
        compiler_params=pltpu.CompilerParams(
            collective_id=0, has_side_effects=True, vmem_limit_bytes=60 << 20
        ),
    )(routes.T, gates.T, norm_gain.reshape(1, -1), tokens, wg, wu, wd, sg, su, sd)
    return mixed, load.reshape(32)


def solution(mesh):
    rows = P(("ep", "tp"), None)
    expert = P("tp", None, None)
    return jax.shard_map(
        per_device,
        mesh=mesh,
        in_specs=(rows, P(), rows, rows, expert, expert, expert, P(), P(), P()),
        out_specs=(rows, P()),
        check_vma=False,
    )
```

time: 123 us -> 96.3 us (0.78)
  Pallas kernels: 116 us -> 92.5 us
  local copies, waits for them, and re-layouts: 5.9 us -> 2.99 us
    pallas_call x1, Pallas kernels: 116 us -> 92.5 us  [per_device(): pl.pallas_call(kernel, out_shape=(jax.ShapeDtypeStruct((128, 2048), BF16)...]
    unnamed x3 -> x2, local copies, waits for them, and re-layouts: 4.71 us -> 2.99 us
where the time goes in v2:
time: 96.3 us; the launch traced here: 96.1 us
  Pallas kernels  92.5 us (96%)
  local copies, waits for them, and re-layouts  2.99 us (3%)
    pallas_call x1, Pallas kernels, per_device(): pl.pallas_call(kernel, out_shape=(jax.ShapeDtypeStruct((128, 2048), BF16)...  92.5 us
    unnamed x2, local copies, waits for them, and re-layouts  2.99 us

profile of v2, /device:TPU:1, one launch (start us, length us, event | category | flops | bytes accessed | tf_op | source)
XLA Modules:
  0.0 96.1 jit_solution(7693859150878756755)
XLA Ops:
  0.6 92.5 %shard_map.113 = (bf16[128,2048]{1,0:T(8,128)(2,1)}, f32[1,32]{1,0:T(1,128)}) custom-call(s32[2,128]{1,0:T(2,128)} %bitcast.5, f32[2,128]{1,0:T(2,128)} %bitcast.6, f32[1,2048]{1,0:T(1,128)} %bitcast.4, bf16[128,2048]{1,0:T(8,128)(2,1)} %tokens_hbm.1, bf16[1,2048,512]{2,1,0:T(8,128)(2,1)} %wg_hbm.1, bf16[1,2048,512]{2,1,0:T(8,128)(2,1)} %wu_hbm.1, ...), custom_call_target="tpu_custom_call" | custom-call | tf_op jit(solution)/shard_map/pallas_call | solution.py:450
  93.1 1.9 %copy.14 = bf16[128,2048]{1,0:T(8,128)(2,1)} copy(bf16[128,2048]{1,0:T(8,128)(2,1)} %get-tuple-element.8) | data formatting | bytes 1048576
  95.0 1.1 %copy.15 = f32[32]{0:T(128)} copy(f32[32]{0:T(128)} %bitcast.7) | data formatting | bytes 256

commit v3 on v1

v3 whole, which is shorter than its diff:
```python
import functools

import jax
import jax.numpy as jnp
from jax import lax
from jax.experimental import pallas as pl
from jax.experimental.pallas import tpu as pltpu
from jax.sharding import PartitionSpec as P

NY, NX, NZ = 8, 4, 12
CAP = 16
MESH = pl.DeviceIdType.MESH
F32, BF16 = jnp.float32, jnp.bfloat16

SHIFTS = (0, -1, 1, -2, 2)
TO_B = 3
FIRST_B = len(SHIFTS) * NX
SLOTS = FIRST_B + TO_B * NX
OFFSETS = [(dy, dx) for dy in SHIFTS + SHIFTS[:TO_B] for dx in range(NX)]
BLOCKS = ((0, 4), (4, 12), (12, 20), (20, 24), (24, 32))
BACK = ((0, 4), (4, 12), (12, 20), (20, 32))
TOTAL = SLOTS * CAP
SUB = 64
PARTS = (4,4)
SUBS = max(PARTS)
SHARE = (PARTS[0] * SUB, PARTS[1] * SUB)
UP = (5, 5, 5, 5, 5, 5, 5, 5, 5, 6, 6, 6)


def kernel(
    routes_hbm,
    gates_hbm,
    gain_hbm,
    tokens_hbm,
    wg_hbm,
    wu_hbm,
    wd_hbm,
    sg_hbm,
    su_hbm,
    sd_hbm,
    mixed_ref,
    load_ref,
    routes_ref,
    gates_ref,
    gain_ref,
    tok,
    normed,
    weights_a,
    weights_b,
    stage,
    sg,
    su,
    sd,
    outgoing,
    arrived,
    result,
    returned,
    hidden,
    shidden,
    acc,
    csrc,
    cz,
    cplane,
    cpair,
    local_sem,
    own_sem,
    stage_sem,
    send_sem,
    recv_sem,
    back_send,
    back_recv,
    csend,
    crecv,
    ysend,
    yrecv,
    zsend,
    zrecv,
    psend,
    precv,
    zready,
    yready,
    all_z,
):
    ep, tp = lax.axis_index("ep"), lax.axis_index("tp")
    my_y, my_x = tp // NX, tp % NX
    my_z, core = ep // 2, ep % 2

    def device(dy=0, dx=0, dz=0):
        return {
            "ep": lax.rem(my_z + dz + NZ, NZ) * 2 + core,
            "tp": lax.rem(my_y + dy + NY, NY) * NX + lax.rem(my_x + dx + NX, NX),
        }

    partner = {"ep": my_z * 2 + 1 - core, "tp": tp}

    def remote(src, dst, send, recv, to):
        return pltpu.make_async_remote_copy(
            src_ref=src, dst_ref=dst, send_sem=send, recv_sem=recv, device_id=to, device_id_type=MESH
        )

    def signal(sem, to):
        pl.semaphore_signal(sem, inc=1, device_id=to, device_id_type=MESH)

    copies = [
        pltpu.make_async_copy(src, dst, local_sem.at[i])
        for i, (src, dst) in enumerate(
            [
                (tokens_hbm, tok),
                (routes_hbm, routes_ref),
                (gates_hbm, gates_ref),
                (gain_hbm, gain_ref),
                (sg_hbm, sg),
                (su_hbm, su),
                (sd_hbm, sd),
            ]
        )
    ]
    quarter = pl.multiple_of(lax.rem(my_z, 4) * 512, 512)
    def each_core(act):
        for c in range(2):

            @pl.when(core == c)
            def _():
                act(c)

    def begin(c):
        return c * SHARE[0]

    def staged(c, part):
        mine = pl.ds(pl.multiple_of(quarter + begin(c), SUB), SHARE[c])
        src = (
            wg_hbm.at[0, mine, :],
            wu_hbm.at[0, mine, :],
            wd_hbm.at[0, begin(c) : begin(c) + SHARE[c], pl.ds(quarter, 512)],
        )[part]
        return pltpu.make_async_copy(src, stage.at[0 : SHARE[c], :], stage_sem)

    for part in range(3):

        @pl.when(my_z // 4 == part)
        def _():
            each_core(lambda c: staged(c, part).start())

    for c in copies[:4]:
        c.start()

    own = [
        pltpu.make_async_copy(wg_hbm.at[0], weights_a.at[0:2048, :], own_sem.at[0]),
        pltpu.make_async_copy(wu_hbm.at[0], weights_a.at[2048:4096, :], own_sem.at[1]),
    ] + [
        pltpu.make_async_copy(
            wd_hbm.at[0, :, k * 512 : (k + 1) * 512],
            weights_a.at[(8 + k) * 512 : (9 + k) * 512, :],
            own_sem.at[2],
        )
        for k in range(4)
    ]
    own_down = pltpu.make_async_copy(wg_hbm.at[0], weights_a.at[4096:6144, :], own_sem.at[2])

    def sub(k, q):
        return weights_b.at[pl.ds(pl.multiple_of(k * 512 + core * SHARE[0] + q * SUB, SUB), SUB), :]

    def across(q):
        return remote(
            stage.at[pl.ds(q * SUB, SUB), :], sub(my_z, q), ysend, yrecv.at[q], device(dy=4)
        )

    def round_z(way, step, q):
        sign = 1 - 2 * way
        at = sub(lax.rem(my_z - sign * (step - 1) + NZ, NZ), q)
        return remote(at, at, zsend, zrecv.at[way, step - 1, q], device(dz=sign))

    def over(way, step, q):
        at = sub(lax.rem(my_z - (1 - 2 * way) * step + NZ, NZ), q)
        return remote(at, at, psend, precv, partner)


    barrier = pltpu.get_barrier_semaphore()
    near = [(dy, dx) for dy in SHIFTS for dx in range(NX) if (dy, dx) != (0, 0)]
    for dy, dx in near:
        signal(barrier, device(dy, dx))
    signal(barrier, partner)

    for d in range(1, NZ):

        @pl.when(my_z + d < NZ)
        def _():
            signal(barrier, device(dz=d))

    @pl.when(my_y < NY // 2)
    def _():
        signal(barrier, device(dy=4))

    for c in own + copies[4:]:
        c.start()

    for c in copies[1:4]:
        c.wait()

    shape = (SLOTS, 128)
    slot = lax.broadcasted_iota(jnp.int32, shape, 0)
    to_b = slot >= FIRST_B
    index = jnp.where(to_b, slot - FIRST_B, slot)
    shift = jnp.zeros(shape, jnp.int32)
    for g, dy in enumerate(SHIFTS):
        shift = jnp.where(index // NX == g, dy + NY, shift)
    shift = jnp.where(to_b, shift + NY // 2, shift)
    expert = (my_y + shift) % NY * NX + (my_x + index % NX) % NX
    routes = [routes_ref[k : k + 1, :] for k in range(2)]
    hot = [(r == expert).astype(F32) for r in routes]
    ti = lax.broadcasted_iota(jnp.int32, (128, 128), 0)
    tj = lax.broadcasted_iota(jnp.int32, (128, 128), 1)
    earlier = jnp.dot(
        (hot[0] + hot[1]).astype(BF16),
        (ti < tj).astype(F32).astype(BF16),
        preferred_element_type=F32,
    )
    at = earlier + (CAP * slot).astype(F32)
    pos_row = [jnp.sum(h * at, axis=0, keepdims=True).astype(jnp.int32) for h in hot]
    pos = [jnp.sum(jnp.where(ti == tj, p, 0), axis=1, keepdims=True) for p in pos_row]
    weight = [
        jnp.sum(jnp.where(ti == tj, gates_ref[k : k + 1, :], 0.0), axis=1, keepdims=True)
        for k in range(2)
    ]
    route_col = [jnp.sum(jnp.where(ti == tj, r, 0), axis=1, keepdims=True) for r in routes]
    counts = jnp.sum(
        (route_col[0] == tj).astype(F32) + (route_col[1] == tj).astype(F32), axis=0, keepdims=True
    )
    csrc[0] = jnp.broadcast_to(counts, (8, 128))

    def enter():
        pl.semaphore_wait(barrier, len(near) + 1 + my_z + (my_y >= NY // 2).astype(jnp.int32))

        @pl.when(my_z > 0)
        def _():
            signal(zready.at[0], device(dz=-1))

        @pl.when(my_z == NZ - 1)
        def _():
            signal(zready.at[1], device(dz=1))

        for d in range(1, NZ):

            @pl.when(my_z >= d)
            def _():
                signal(all_z, device(dz=-d))

    def has(q):
        return functools.reduce(jnp.logical_or, [core == c for c in range(2) if q < PARTS[c]])

    def send_across():
        each_core(lambda c: staged(c, 0).wait())
        for q in range(SUBS):

            @pl.when(has(q))
            def _():
                across(q).start()

    @pl.when(my_y >= NY // 2)
    def _():
        enter()
        signal(yready, device(dy=4))
        send_across()

    copies[0].wait()
    gain = gain_ref[...]

    def norm(i, carry):
        rows = pl.ds(pl.multiple_of(i * 16, 16), 16)
        values = tok[rows, :].astype(F32)
        values = values - jnp.mean(values, axis=-1, keepdims=True)
        spread = jnp.mean(values * values, axis=-1, keepdims=True)
        normed[rows, :] = (values * lax.rsqrt(spread + 1e-05) * gain).astype(BF16)
        return carry

    lax.fori_loop(0, 8, norm, 0)

    def build(b):
        rows = slice(b * 128, (b + 1) * 128)
        pick = (ti + b * 128 == pos_row[0]) | (ti + b * 128 == pos_row[1])
        pick = jnp.where(pick, 1.0, 0.0).astype(BF16)
        for n in range(4):
            cols = slice(n * 512, (n + 1) * 512)
            outgoing[rows, cols] = jnp.dot(
                pick, normed[:, cols], preferred_element_type=F32
            ).astype(BF16)

    def rows_of(j):
        return slice(j * CAP, (j + 1) * CAP)

    def block_in(blocks, j):
        return [a <= j < b for a, b in blocks].index(True)

    def dispatch(j):
        dy, dx = OFFSETS[j]
        return remote(
            outgoing.at[rows_of(j), :],
            arrived.at[rows_of(j), :],
            send_sem,
            recv_sem.at[block_in(BLOCKS, j)],
            device(dy, dx),
        )

    def give_back(j):
        dy, dx = OFFSETS[j]
        return remote(
            result.at[rows_of(j), :],
            returned.at[rows_of(j), :],
            back_send,
            back_recv.at[block_in(BACK, j)],
            device(-dy, -dx),
        )

    def away(a, b):
        return [j for j in range(a, b) if OFFSETS[j] != (0, 0)]

    def wait_recv(n, sem):
        some = arrived.at[0 : n * CAP, :]
        remote(some, some, send_sem, sem, device(dy=1)).wait_recv()

    def wait_send(n, sem):
        some = arrived.at[0 : n * CAP, :]
        remote(some, some, sem, recv_sem.at[0], device(dy=1)).wait_send()

    others = [(dy, dx) for dy in range(NY) for dx in range(NX) if (dy, dx) != (0, 0)]

    def count_plane(i):
        return remote(csrc.at[0], cplane.at[i], csend, crecv.at[0], device(*others[i]))

    def count_z(i):
        return remote(csrc.at[1], cz.at[i], csend, crecv.at[1], device(dz=i + 1))

    def count_over():
        return remote(csrc.at[2], cpair, csend, crecv.at[2], partner)

    def wait_counts(ref, n, stage_at):
        some = ref.at[0:n]
        remote(some, some, csend, crecv.at[stage_at], device(dz=1)).wait_recv()
        total = csrc[stage_at]
        for i in range(n):
            total = total + ref[i]
        csrc[stage_at + 1] = total

    build(0)
    arrived[rows_of(0), :] = outgoing[rows_of(0), :]
    build(1)
    build(2)
    arrived[rows_of(FIRST_B), :] = outgoing[rows_of(FIRST_B), :]

    @pl.when(my_y < NY // 2)
    def _():
        enter()
        pl.semaphore_wait(yready, 1)
        signal(yready, device(dy=4))
        send_across()

    for j in away(0, 24):
        dispatch(j).start()
    build(3)
    for j in away(24, 32):
        dispatch(j).start()

    for c in copies[4:]:
        c.wait()
    gate = jnp.dot(normed[...], sg[...], preferred_element_type=F32)
    up = jnp.dot(normed[...], su[...], preferred_element_type=F32)
    shidden[...] = (gate / (1.0 + jnp.exp(-gate)) * up).astype(BF16)
    for n in range(4):
        cols = slice(n * 512, (n + 1) * 512)
        acc[:, cols] = jnp.dot(shidden[...], sd[:, cols], preferred_element_type=F32)

    def arrivals(i):
        wait_recv(len(away(*BLOCKS[i])), recv_sem.at[i])

    def serve(first, end, weights):
        rows = slice(first * CAP, end * CAP)
        m = (end - first) * CAP
        for n in range(2):
            cols = slice(n * 256, (n + 1) * 256)
            gate = jnp.zeros((m, 256), F32)
            up = jnp.zeros((m, 256), F32)
            for k in range(4):
                x = arrived[rows, k * 512 : (k + 1) * 512]
                gate = gate + jnp.dot(
                    x, weights[k * 512 : (k + 1) * 512, cols], preferred_element_type=F32
                )
                up = up + jnp.dot(
                    x, weights[2048 + k * 512 : 2048 + (k + 1) * 512, cols], preferred_element_type=F32
                )
            hidden[0:m, cols] = (gate / (1.0 + jnp.exp(-gate)) * up).astype(BF16)
        for n in range(4):
            cols = slice(n * 512, (n + 1) * 512)
            result[rows, cols] = jnp.dot(
                hidden[0:m, :],
                weights[4096 + n * 512 : 4096 + (n + 1) * 512, :],
                preferred_element_type=F32,
            ).astype(BF16)
        for j in range(first, end):
            if OFFSETS[j] == (0, 0):
                returned[rows_of(j), :] = result[rows_of(j), :]
            else:
                give_back(j).start()

    def own_weights():
        for c in own[:2]:
            c.wait()
        own_down.wait()

    def from_y(q):
        @pl.when(has(q))
        def _():
            across(q).wait_recv()
            remote(sub(my_z, q), sub(my_z, q), psend, precv, partner).start()

        if q == 0:

            @pl.when(my_z < NZ - 1)
            def _():
                pl.semaphore_wait(zready.at[0], 1)

        @pl.when(has(q))
        def _():
            round_z(0, 1, q).start()

        @pl.when(jnp.logical_and(my_z > 0, has(q)))
        def _():
            round_z(1, 1, q).start()

        if q == 0:
            @pl.when(my_y >= NY // 2)
            def _():
                pl.semaphore_wait(yready, 1)

            for i in range(len(others)):
                count_plane(i).start()

    def first_down():
        @pl.when(my_z == 0)
        def _():
            pl.semaphore_wait(zready.at[1], 1)
            for q in range(SUBS):

                @pl.when(has(q))
                def _():
                    round_z(1, 1, q).start()

    def any_of(planes):
        hits = [my_z == z for z in range(NZ) if z in planes]
        if len(hits) > NZ // 2:
            return jnp.logical_not(any_of([z for z in range(NZ) if z not in planes]))
        return functools.reduce(jnp.logical_or, hits, my_z < 0)

    def pass_on(way, step, q, planes):
        goes_on = [
            z
            for z in planes
            if step < (UP[(z - step) % NZ] if way == 0 else NZ - 1 - UP[(z + step) % NZ])
        ]

        @pl.when(jnp.logical_and(any_of(planes), has(q)))
        def _():
            round_z(way, step, q).wait_recv()

            @pl.when(any_of(goes_on))
            def _():
                round_z(way, step + 1, q).start()

            over(way, step, q).start()

    def settle_plane():
        wait_counts(cplane, len(others), 0)

        @pl.when(my_z < NZ - 1)
        def _():
            pl.semaphore_wait(all_z, NZ - 1 - my_z)

        for i in range(NZ - 1):
            count_z(i).start()

    def serve_a(i):
        arrivals(i)
        serve(*BLOCKS[i], weights_a)

    due = [
        (12.0, functools.partial(serve_a, 0)),
        (31.0, functools.partial(serve_a, 1)),
        (39.0, functools.partial(serve_a, 2)),
        (44.0, settle_plane),
        (12.0 + 9.4, first_down),
    ]
    for q in range(SUBS):
        due.append((12.0 + 2.2 * q, functools.partial(from_y, q)))
        for step in range(1, NZ // 2 + 1):
            usual = 12.0 + 5.65 * (step - 1) + (2.2 - 0.39375000000000004 * min(step - 1, 2)) * q
            down = [z for z in range(NZ) if step <= NZ - 1 - UP[(z + step) % NZ]]
            due.append((usual + 5.0, functools.partial(pass_on, 1, step, q, [z for z in down if z > 0])))
            if 0 in down:
                due.append((usual + 9.5, functools.partial(pass_on, 1, step, q, [0])))
            up = [z for z in range(NZ) if step <= UP[(z - step) % NZ]]
            due.append((usual + 3.0, functools.partial(pass_on, 0, step, q, [z for z in up if z >= step])))
            for z in up:
                if z < step:
                    due.append((usual + 3.0 + max(0.0, 12.5 - 2.5 * z), functools.partial(pass_on, 0, step, q, [z])))
    own_weights()
    for _, act in sorted(due, key=lambda d: d[0]):
        act()

    arrivals(3)
    arrivals(4)
    def bytes_of(rows, c, n):
        return rows.at[0 : n * SHARE[c], :]

    def other_part(c):
        some = bytes_of(weights_b, 1 - c, 12)
        remote(some, some, psend, precv, partner).wait_recv()

    each_core(other_part)
    serve(FIRST_B, SLOTS, weights_b)

    for i, (first, end) in enumerate(BACK):
        rows = slice(first * CAP, end * CAP)
        m = (end - first) * CAP
        where = lax.broadcasted_iota(jnp.int32, (128, m), 1) + first * CAP
        pick = jnp.concatenate(
            [jnp.where(where == p, 1.0, 0.0).astype(BF16) for p in pos], axis=0
        )
        if i == len(BACK) - 1:
            wait_counts(cz, NZ - 1, 1)
            count_over().start()
        wait_recv(len(away(first, end)), back_recv.at[i])
        for n in range(4):
            cols = slice(n * 512, (n + 1) * 512)
            pair = jnp.dot(pick, returned[rows, cols], preferred_element_type=F32)
            total = acc[:, cols] + (weight[0] * pair[:128] + weight[1] * pair[128:])
            if i + 1 < len(BACK):
                acc[:, cols] = total
            else:
                mixed_ref[:, cols] = total.astype(BF16)

    count_over().wait_recv()

    load_ref[...] = (csrc[2, 0:1, 0:32] + cpair[0:1, 0:32]) * (32 / 196608)

    wait_send(len(away(0, SLOTS)), send_sem)
    wait_send(len(away(0, SLOTS)), back_send)
    def passed(z):
        ups = sum(step <= UP[(z + 1 - step) % NZ] for step in range(1, NZ))
        downs = sum(step <= NZ - 1 - UP[(z - 1 + step) % NZ] for step in range(1, NZ))
        return ups + downs

    def weights_left(c):
        some = bytes_of(stage, c, 1)
        remote(some, some, ysend, yrecv.at[0], device(dy=4)).wait_send()
        some = bytes_of(weights_b, c, 12)
        remote(some, some, psend, precv, partner).wait_send()
        for n in sorted({passed(z) for z in range(NZ)}):

            @pl.when(any_of([z for z in range(NZ) if passed(z) == n]))
            def _():
                some = bytes_of(weights_b, c, n)
                remote(some, some, zsend, zrecv.at[0, 0, 0], device(dz=1)).wait_send()

    each_core(weights_left)
    some = cplane.at[0 : 11 + len(others) + 1]
    remote(some, some, csend, crecv.at[0], device(dz=1)).wait_send()


def per_device(tokens, norm_gain, routes, gates, wg, wu, wd, sg, su, sd):
    vmem = pl.BlockSpec(memory_space=pltpu.VMEM)
    anywhere = pl.BlockSpec(memory_space=pl.ANY)
    dma = pltpu.SemaphoreType.DMA
    regular = pltpu.SemaphoreType.REGULAR
    mixed, load = pl.pallas_call(
        kernel,
        out_shape=(
            pltpu.VMEM((128, 2048), BF16),
            pltpu.VMEM((1, 32), F32),
        ),
        in_specs=[anywhere] * 10,
        out_specs=(vmem, vmem),
        scratch_shapes=[
            pltpu.VMEM((2, 128), jnp.int32),
            pltpu.VMEM((2, 128), F32),
            pltpu.VMEM((1, 2048), F32),
            pltpu.VMEM((128, 2048), BF16),
            pltpu.VMEM((128, 2048), BF16),
            pltpu.VMEM((12 * 512, 512), BF16),
            pltpu.VMEM((12 * 512, 512), BF16),
            pltpu.VMEM((max(SHARE), 512), BF16),
            pltpu.VMEM((2048, 256), BF16),
            pltpu.VMEM((2048, 256), BF16),
            pltpu.VMEM((256, 2048), BF16),
            pltpu.VMEM((TOTAL, 2048), BF16),
            pltpu.VMEM((TOTAL, 2048), BF16),
            pltpu.VMEM((TOTAL, 2048), BF16),
            pltpu.VMEM((TOTAL, 2048), BF16),
            pltpu.VMEM((192, 512), BF16),
            pltpu.VMEM((128, 256), BF16),
            pltpu.VMEM((128, 2048), F32),
            pltpu.VMEM((3, 8, 128), F32),
            pltpu.VMEM((NZ - 1, 8, 128), F32),
            pltpu.VMEM((48, 8, 128), F32),
            pltpu.VMEM((8, 128), F32),
            dma((7,)),
            dma((3,)),
            dma(()),
            dma(()),
            dma((len(BLOCKS),)),
            dma(()),
            dma((len(BACK),)),
            dma(()),
            dma((3,)),
            dma(()),
            dma((SUBS,)),
            dma(()),
            dma((2, 6, SUBS)),
            dma(()),
            dma(()),
            regular((2,)),
            regular,
            regular,
        ],
        compiler_params=pltpu.CompilerParams(
            collective_id=0, has_side_effects=True, vmem_limit_bytes=60 << 20
        ),
    )(routes.T, gates.T, norm_gain.reshape(1, -1), tokens, wg, wu, wd, sg, su, sd)
    return mixed, load.reshape(32)


def solution(mesh):
    rows = P(("ep", "tp"), None)
    expert = P("tp", None, None)
    return jax.shard_map(
        per_device,
        mesh=mesh,
        in_specs=(rows, P(), rows, rows, expert, expert, expert, P(), P(), P()),
        out_specs=(rows, P()),
        check_vma=False,
    )
```

time: 123 us -> 78.2 us (0.64)
  the two profiles are of different devices: /device:TPU:1 before, /device:TPU:65 now
where the time goes in v3:
time: 78.2 us; the launch traced here: 78.1 us
  Pallas kernels  76.2 us (97%)
  local copies, waits for them, and re-layouts  1.31 us (2%)
    pallas_call x1, Pallas kernels, per_device(): pl.pallas_call(kernel, out_shape=(pltpu.VMEM((128, 2048), BF16), pltpu.VM...  76.2 us

profile of v3, /device:TPU:65, one launch (start us, length us, event | category | flops | bytes accessed | tf_op | source)
XLA Modules:
  0.0 78.1 jit_solution(4077623102839759196)
XLA Ops:
  0.6 76.2 %shard_map.113 = (bf16[128,2048]{1,0:T(8,128)(2,1)S(1)}, f32[1,32]{1,0:T(1,128)S(1)}) custom-call(s32[2,128]{1,0:T(2,128)} %bitcast.6, f32[2,128]{1,0:T(2,128)} %bitcast.7, f32[1,2048]{1,0:T(1,128)} %bitcast.5, bf16[128,2048]{1,0:T(8,128)(2,1)} %tokens_hbm.1, bf16[1,2048,512]{2,1,0:T(8,128)(2,1)} %wg_hbm.1, bf16[1,2048,512]{2,1,0:T(8,128)(2,1)} %wu_hbm.1, ...), custom_call_target="tpu_custom_call" | custom-call | tf_op jit(solution)/shard_map/pallas_call | solution.py:573
  76.8 0.8 %copy.14 = bf16[128,2048]{1,0:T(8,128)(2,1)} copy(bf16[128,2048]{1,0:T(8,128)(2,1)S(1)} %get-tuple-element.6) | data formatting | bytes 1048576
  77.6 0.5 copy.15

commit v4 on v3

--- a/solution.py
+++ b/solution.py
@@ -12,18 +12,20 @@
 MESH = pl.DeviceIdType.MESH
 F32, BF16 = jnp.float32, jnp.bfloat16
 
-SHIFTS = (0, -1, 1, -2, 2)
-TO_B = 3
-FIRST_B = len(SHIFTS) * NX
-SLOTS = FIRST_B + TO_B * NX
-OFFSETS = [(dy, dx) for dy in SHIFTS + SHIFTS[:TO_B] for dx in range(NX)]
-BLOCKS = ((0, 4), (4, 12), (12, 20), (20, 24), (24, 32))
+TO_A = (0, -1, 1, -2, 2)
+TO_B = (0, -1, 1)
+FIRST_B = len(TO_A) * NX
+SLOTS = FIRST_B + len(TO_B) * NX
+OFFSETS = [(dy, dx) for dy in TO_A + TO_B for dx in range(NX)]
+SELF_A, SELF_B = FIRST_B - NX * (len(TO_A) - TO_A.index(0)), FIRST_B + NX * TO_B.index(0)
+BLOCKS = ((0, 4), (4, 12), (12, 20), (20, 32))
 BACK = ((0, 4), (4, 12), (12, 20), (20, 32))
 TOTAL = SLOTS * CAP
 SUB = 64
 PARTS = (4,4)
 SUBS = max(PARTS)
 SHARE = (PARTS[0] * SUB, PARTS[1] * SUB)
+SLOW_TO = 10
 UP = (5, 5, 5, 5, 5, 5, 5, 5, 5, 6, 6, 6)
 
 
@@ -176,14 +178,22 @@
 
 
     barrier = pltpu.get_barrier_semaphore()
-    near = [(dy, dx) for dy in SHIFTS for dx in range(NX) if (dy, dx) != (0, 0)]
+    near = [(dy, dx) for dy in TO_A for dx in range(NX) if (dy, dx) != (0, 0)]
     for dy, dx in near:
         signal(barrier, device(dy, dx))
     signal(barrier, partner)
 
+    first = jnp.logical_and(tp == 0, core == 0)
+    slow = jnp.logical_and(first, my_z == 0)
+    over_slow = jnp.logical_and(first, jnp.logical_and(my_z > 0, my_z < SLOW_TO))
+
+    @pl.when(over_slow)
+    def _():
+        signal(barrier, {"ep": core, "tp": tp})
+
     for d in range(1, NZ):
 
-        @pl.when(my_z + d < NZ)
+        @pl.when(jnp.logical_and(my_z + d < NZ, jnp.logical_not(jnp.logical_and(slow, d < SLOW_TO))))
         def _():
             signal(barrier, device(dz=d))
 
@@ -199,13 +209,10 @@
 
     shape = (SLOTS, 128)
     slot = lax.broadcasted_iota(jnp.int32, shape, 0)
-    to_b = slot >= FIRST_B
-    index = jnp.where(to_b, slot - FIRST_B, slot)
     shift = jnp.zeros(shape, jnp.int32)
-    for g, dy in enumerate(SHIFTS):
-        shift = jnp.where(index // NX == g, dy + NY, shift)
-    shift = jnp.where(to_b, shift + NY // 2, shift)
-    expert = (my_y + shift) % NY * NX + (my_x + index % NX) % NX
+    for g, dy in enumerate(TO_A + tuple(dy + NY // 2 for dy in TO_B)):
+        shift = jnp.where(slot // NX == g, dy + NY, shift)
+    expert = (my_y + shift) % NY * NX + (my_x + slot % NX) % NX
     routes = [routes_ref[k : k + 1, :] for k in range(2)]
     hot = [(r == expert).astype(F32) for r in routes]
     ti = lax.broadcasted_iota(jnp.int32, (128, 128), 0)
@@ -229,9 +236,17 @@
     csrc[0] = jnp.broadcast_to(counts, (8, 128))
 
     def enter():
-        pl.semaphore_wait(barrier, len(near) + 1 + my_z + (my_y >= NY // 2).astype(jnp.int32))
-
-        @pl.when(my_z > 0)
+        early = my_z + (my_y >= NY // 2).astype(jnp.int32)
+        early = early + jnp.where(slow, SLOW_TO - 1, 0) - over_slow.astype(jnp.int32)
+        pl.semaphore_wait(barrier, len(near) + 1 + early)
+
+        @pl.when(slow)
+        def _():
+            signal(zready.at[1], device(dz=1))
+            for d in range(1, SLOW_TO):
+                signal(all_z, device(dz=d))
+
+        @pl.when(jnp.logical_and(my_z > 0, jnp.logical_not(jnp.logical_and(over_slow, my_z == 1))))
         def _():
             signal(zready.at[0], device(dz=-1))
 
@@ -241,7 +256,7 @@
 
         for d in range(1, NZ):
 
-            @pl.when(my_z >= d)
+            @pl.when(jnp.logical_and(my_z >= d, jnp.logical_not(jnp.logical_and(over_slow, my_z == d))))
             def _():
                 signal(all_z, device(dz=-d))
 
@@ -273,7 +288,7 @@
         normed[rows, :] = (values * lax.rsqrt(spread + 1e-05) * gain).astype(BF16)
         return carry
 
-    lax.fori_loop(0, 8, norm, 0)
+    lax.fori_loop(0, 8, norm, 0, unroll=2)
 
     def build(b):
         rows = slice(b * 128, (b + 1) * 128)
@@ -341,24 +356,29 @@
             total = total + ref[i]
         csrc[stage_at + 1] = total
 
-    build(0)
-    arrived[rows_of(0), :] = outgoing[rows_of(0), :]
-    build(1)
-    build(2)
-    arrived[rows_of(FIRST_B), :] = outgoing[rows_of(FIRST_B), :]
+    for b in (0, 2, 1, 3):
+        build(b)
+    for j in (SELF_A, SELF_B):
+        arrived[rows_of(j), :] = outgoing[rows_of(j), :]
 
     @pl.when(my_y < NY // 2)
     def _():
         enter()
+
+    own_row = [j for j in range(SLOTS) if OFFSETS[j][0] == 0]
+    for j in own_row:
+        if j not in (SELF_A, SELF_B):
+            dispatch(j).start()
+
+    @pl.when(my_y < NY // 2)
+    def _():
         pl.semaphore_wait(yready, 1)
         signal(yready, device(dy=4))
         send_across()
 
-    for j in away(0, 24):
-        dispatch(j).start()
-    build(3)
-    for j in away(24, 32):
-        dispatch(j).start()
+    for j in range(FIRST_B):
+        if j not in own_row:
+            dispatch(j).start()
 
     for c in copies[4:]:
         c.wait()
@@ -414,9 +434,13 @@
 
         if q == 0:
 
-            @pl.when(my_z < NZ - 1)
+            @pl.when(jnp.logical_and(my_z < NZ - 1, jnp.logical_not(slow)))
             def _():
                 pl.semaphore_wait(zready.at[0], 1)
+
+            @pl.when(jnp.logical_and(over_slow, my_z == 1))
+            def _():
+                pl.semaphore_wait(zready.at[1], 1)
 
         @pl.when(has(q))
         def _():
@@ -472,7 +496,8 @@
 
         @pl.when(my_z < NZ - 1)
         def _():
-            pl.semaphore_wait(all_z, NZ - 1 - my_z)
+            answers = NZ - 1 - my_z + over_slow.astype(jnp.int32) - jnp.where(slow, SLOW_TO - 1, 0)
+            pl.semaphore_wait(all_z, answers)
 
         for i in range(NZ - 1):
             count_z(i).start()
@@ -481,8 +506,14 @@
         arrivals(i)
         serve(*BLOCKS[i], weights_a)
 
+    def send_b():
+        for j in range(FIRST_B, SLOTS):
+            if j not in own_row:
+                dispatch(j).start()
+
     due = [
-        (12.0, functools.partial(serve_a, 0)),
+        (12.5, send_b),
+(12.0, functools.partial(serve_a, 0)),
         (31.0, functools.partial(serve_a, 1)),
         (39.0, functools.partial(serve_a, 2)),
         (44.0, settle_plane),
@@ -506,7 +537,6 @@
         act()
 
     arrivals(3)
-    arrivals(4)
     def bytes_of(rows, c, n):
         return rows.at[0 : n * SHARE[c], :]
 
@@ -515,7 +545,7 @@
         remote(some, some, psend, precv, partner).wait_recv()
 
     each_core(other_part)
-    serve(FIRST_B, SLOTS, weights_b)
+    serve(*BLOCKS[-1], weights_b)
 
     for i, (first, end) in enumerate(BACK):
         rows = slice(first * CAP, end * CAP)

time: 78.2 us -> 77.5 us (level)
  the two profiles are of different devices: /device:TPU:65 before, /device:TPU:1 now
where the time goes in v4:
time: 77.5 us; the launch traced here: 76.5 us
  Pallas kernels  74.5 us (96%)
  local copies, waits for them, and re-layouts  1.31 us (2%)
    pallas_call x1, Pallas kernels, per_device(): pl.pallas_call(kernel, out_shape=(pltpu.VMEM((128, 2048), BF16), pltpu.VM...  74.5 us

profile of v4, /device:TPU:1, one launch (start us, length us, event | category | flops | bytes accessed | tf_op | source)
XLA Modules:
  0.0 76.5 jit_solution(352136903352479058)
XLA Ops:
  0.6 74.5 %shard_map.113 = (bf16[128,2048]{1,0:T(8,128)(2,1)S(1)}, f32[1,32]{1,0:T(1,128)S(1)}) custom-call(s32[2,128]{1,0:T(2,128)} %bitcast.6, f32[2,128]{1,0:T(2,128)} %bitcast.7, f32[1,2048]{1,0:T(1,128)} %bitcast.5, bf16[128,2048]{1,0:T(8,128)(2,1)} %tokens_hbm.1, bf16[1,2048,512]{2,1,0:T(8,128)(2,1)} %wg_hbm.1, bf16[1,2048,512]{2,1,0:T(8,128)(2,1)} %wu_hbm.1, ...), custom_call_target="tpu_custom_call" | custom-call | tf_op jit(solution)/shard_map/pallas_call | solution.py:603
  75.2 0.8 %copy.14 = bf16[128,2048]{1,0:T(8,128)(2,1)} copy(bf16[128,2048]{1,0:T(8,128)(2,1)S(1)} %get-tuple-element.6) | data formatting | bytes 1048576
  76.0 0.5 copy.15

commit v5 on v4

--- a/solution.py
+++ b/solution.py
@@ -19,7 +19,7 @@
 OFFSETS = [(dy, dx) for dy in TO_A + TO_B for dx in range(NX)]
 SELF_A, SELF_B = FIRST_B - NX * (len(TO_A) - TO_A.index(0)), FIRST_B + NX * TO_B.index(0)
 BLOCKS = ((0, 4), (4, 12), (12, 20), (20, 32))
-BACK = ((0, 4), (4, 12), (12, 20), (20, 32))
+BACK = ((0, 4), (4, 12), (12, 20), (20, 24), (24, 32))
 TOTAL = SLOTS * CAP
 SUB = 64
 PARTS = (4,4)
@@ -365,7 +365,7 @@
     def _():
         enter()
 
-    own_row = [j for j in range(SLOTS) if OFFSETS[j][0] == 0]
+    own_row = [j for j in range(FIRST_B) if OFFSETS[j][0] == 0]
     for j in own_row:
         if j not in (SELF_A, SELF_B):
             dispatch(j).start()
@@ -415,7 +415,7 @@
                 weights[4096 + n * 512 : 4096 + (n + 1) * 512, :],
                 preferred_element_type=F32,
             ).astype(BF16)
-        for j in range(first, end):
+        for j in reversed(range(first, end)):
             if OFFSETS[j] == (0, 0):
                 returned[rows_of(j), :] = result[rows_of(j), :]
             else:
@@ -507,8 +507,8 @@
         serve(*BLOCKS[i], weights_a)
 
     def send_b():
-        for j in range(FIRST_B, SLOTS):
-            if j not in own_row:
+        for j in [*range(FIRST_B + NX, SLOTS), *range(FIRST_B + 1, FIRST_B + NX)]:
+            if j != SELF_B:
                 dispatch(j).start()
 
     due = [

time: 77.5 us -> 77.3 us (level)
  no operation moved by 1% of the time
where the time goes in v5:
time: 77.3 us; the launch traced here: 76.9 us
  Pallas kernels  74.9 us (97%)
  local copies, waits for them, and re-layouts  1.31 us (2%)
    pallas_call x1, Pallas kernels, per_device(): pl.pallas_call(kernel, out_shape=(pltpu.VMEM((128, 2048), BF16), pltpu.VM...  74.9 us

profile of v5, /device:TPU:1, one launch (start us, length us, event | category | flops | bytes accessed | tf_op | source)
XLA Modules:
  0.0 76.9 jit_solution(5343136456609960796)
XLA Ops:
  0.6 74.9 %shard_map.113 = (bf16[128,2048]{1,0:T(8,128)(2,1)S(1)}, f32[1,32]{1,0:T(1,128)S(1)}) custom-call(s32[2,128]{1,0:T(2,128)} %bitcast.6, f32[2,128]{1,0:T(2,128)} %bitcast.7, f32[1,2048]{1,0:T(1,128)} %bitcast.5, bf16[128,2048]{1,0:T(8,128)(2,1)} %tokens_hbm.1, bf16[1,2048,512]{2,1,0:T(8,128)(2,1)} %wg_hbm.1, bf16[1,2048,512]{2,1,0:T(8,128)(2,1)} %wu_hbm.1, ...), custom_call_target="tpu_custom_call" | custom-call | tf_op jit(solution)/shard_map/pallas_call | solution.py:603
  75.5 0.8 %copy.14 = bf16[128,2048]{1,0:T(8,128)(2,1)} copy(bf16[128,2048]{1,0:T(8,128)(2,1)S(1)} %get-tuple-element.6) | data formatting | bytes 1048576
  76.3 0.5 copy.15

commit v6 on v5

--- a/solution.py
+++ b/solution.py
@@ -376,7 +376,7 @@
         signal(yready, device(dy=4))
         send_across()
 
-    for j in range(FIRST_B):
+    for j in [g * NX + dx for g in range(len(TO_A)) for dx in reversed(range(NX))]:
         if j not in own_row:
             dispatch(j).start()
 

time: 77.3 us -> 77.3 us (level)
  no operation moved by 1% of the time
where the time goes in v6:
time: 77.3 us; the launch traced here: 76.1 us
  Pallas kernels  74.2 us (96%)
  local copies, waits for them, and re-layouts  1.31 us (2%)
    pallas_call x1, Pallas kernels, per_device(): pl.pallas_call(kernel, out_shape=(pltpu.VMEM((128, 2048), BF16), pltpu.VM...  74.2 us

profile of v6, /device:TPU:1, one launch (start us, length us, event | category | flops | bytes accessed | tf_op | source)
XLA Modules:
  0.0 76.1 jit_solution(12802487473303811757)
XLA Ops:
  0.6 74.2 %shard_map.113 = (bf16[128,2048]{1,0:T(8,128)(2,1)S(1)}, f32[1,32]{1,0:T(1,128)S(1)}) custom-call(s32[2,128]{1,0:T(2,128)} %bitcast.6, f32[2,128]{1,0:T(2,128)} %bitcast.7, f32[1,2048]{1,0:T(1,128)} %bitcast.5, bf16[128,2048]{1,0:T(8,128)(2,1)} %tokens_hbm.1, bf16[1,2048,512]{2,1,0:T(8,128)(2,1)} %wg_hbm.1, bf16[1,2048,512]{2,1,0:T(8,128)(2,1)} %wu_hbm.1, ...), custom_call_target="tpu_custom_call" | custom-call | tf_op jit(solution)/shard_map/pallas_call | solution.py:603
  74.8 0.8 %copy.14 = bf16[128,2048]{1,0:T(8,128)(2,1)} copy(bf16[128,2048]{1,0:T(8,128)(2,1)S(1)} %get-tuple-element.6) | data formatting | bytes 1048576
  75.6 0.5 copy.15
